TPU v7x, 32 devices: a whole 2x2x4 slice. The times are simulated.
32 devices in a mesh: ep: 8 (over z, core), tp: 4 (over y, x).
Axes of the slice: x: 2, y: 2, z: 4, core: 2. Of those that a mesh axis runs over, the one named last changes fastest.
Arguments:
- hidden: bfloat16 [96, 2048], P('ep'), may hold values from -6 to 6
- pre_gain: bfloat16 [2048], replicated, may hold values from 0.099609375 to 1.8984375
- query_weight: bfloat16 [2048, 1024], P('ep', 'tp'), may hold values from -0.125 to 0.125
- key_cache: bfloat16 [96, 1024, 1024], P('ep', 'tp'), may hold values from -6 to 6
- value_cache: bfloat16 [96, 1024, 1024], P('ep', 'tp'), may hold values from -6 to 6
- lengths: int32 [96], P('ep'), may hold values from 128 to 1024
- stick_bias: float32 [16], P('tp'), may hold values from -8.5 to -3
- out_weight: bfloat16 [1024, 2048], P('tp', 'ep'), may hold values from -0.1875 to 0.1875
- post_gain: bfloat16 [2048], replicated, may hold values from 0.099609375 to 1.8984375
- ffn_gain: bfloat16 [2048], replicated, may hold values from 0.099609375 to 1.8984375
- expert_ids: int32 [96, 2], P('ep'), may hold values from 0 to 7, as said below
- route_logits: float32 [96, 2], P('ep'), may hold values from -6 to 6
- gate_experts: bfloat16 [8, 2048, 2048], P('ep', None, 'tp'), may hold values from -0.125 to 0.125
- up_experts: bfloat16 [8, 2048, 2048], P('ep', None, 'tp'), may hold values from -0.125 to 0.125
- down_experts: bfloat16 [8, 2048, 2048], P('ep', 'tp'), may hold values from -2 to 2
- out_gain: bfloat16 [2048], P('tp'), may hold values from 0.099609375 to 1.8984375
Outputs:
- result: bfloat16 [96, 2048], P('ep', 'tp')
Inputs may be any that keep to these rules, and one draw needn't show every extreme that they name: `expert_ids`: each row names 2 different experts of one group of 4 consecutive experts. Among the rows of one device (aligned blocks of 12 rows) no expert is named more than 6 times, and one expert is named exactly 6 times in every block.
All inputs are finite; a program needn't handle non-finite values.
Results may differ from a plain program's by a relative error of at most 0.014.
Values may be sent and summed in bfloat16 or wider, within the bound.
No kernel may reach another device: no remote copies, remote signals or barrier semaphores. Data moves between devices by JAX's collectives and lax.ppermute only.
A program may use at most 64 MiB of HBM per device.

v0:
```python
import jax
import jax.numpy as jnp
from jax import lax
from jax.sharding import PartitionSpec as P

epsilon = 1e-06


def inverse_rms(squares, features):
    return lax.rsqrt(squares / features + epsilon)


def stick_read(queries, key_blocks, value_blocks, lengths, head_bias):
    sequences, heads, head_size = queries.shape
    positions = key_blocks.shape[3]
    scores = jnp.einsum("she,shec->shc", queries, key_blocks, preferred_element_type=jnp.float32)
    scores = scores * head_size ** (-0.5) + head_bias[None, :, None]
    places = lax.broadcasted_iota(jnp.int32, (sequences, heads, positions), 2)
    inside = places < lengths[:, None, None]
    log_fail = jnp.where(inside, jax.nn.log_sigmoid(-scores), 0.0)
    after_sum = lax.cumsum(log_fail, axis=2, reverse=True) - log_fail
    weight = jnp.where(inside, jnp.exp(jax.nn.log_sigmoid(scores) + after_sum), 0.0).astype(
        jnp.bfloat16
    )
    mixed_heads = jnp.einsum(
        "shc,shec->she", weight, value_blocks, preferred_element_type=jnp.float32
    )
    return mixed_heads.astype(jnp.bfloat16)


def per_device(
    hidden,
    pre_gain,
    query_weight,
    key_cache,
    value_cache,
    lengths,
    stick_bias,
    out_weight,
    post_gain,
    ffn_gain,
    expert_ids,
    route_logits,
    gate_experts,
    up_experts,
    down_experts,
    out_gain,
):
    sequences, features = hidden.shape
    ep_count = lax.axis_size("ep")
    tp_count = lax.axis_size("tp")
    tp_place = lax.axis_index("tp")
    heads_here = stick_bias.shape[0]
    head_size = key_cache.shape[1] // heads_here
    positions = key_cache.shape[2]
    slice_width = features // tp_count
    hidden_wide = hidden.astype(jnp.float32)
    normed = (
        hidden_wide
        * inverse_rms(jnp.sum(hidden_wide * hidden_wide, axis=1, keepdims=True), features)
        * pre_gain.astype(jnp.float32)
    ).astype(jnp.bfloat16)
    queries = jnp.dot(
        normed,
        lax.all_gather(query_weight, "ep", axis=0, tiled=True),
        preferred_element_type=jnp.float32,
    )
    queries = queries.astype(jnp.bfloat16).reshape(sequences, heads_here, head_size)
    key_blocks = key_cache.reshape(sequences, heads_here, head_size, positions)
    value_blocks = value_cache.reshape(sequences, heads_here, head_size, positions)
    mixed_heads = stick_read(queries, key_blocks, value_blocks, lengths, stick_bias)
    mixed_heads = mixed_heads.reshape(sequences, heads_here * head_size)
    partial_value = jnp.dot(
        mixed_heads,
        lax.all_gather(out_weight, "ep", axis=1, tiled=True),
        preferred_element_type=jnp.float32,
    )
    attended = lax.psum(partial_value, "tp").astype(jnp.bfloat16)
    attended = lax.optimization_barrier(attended).astype(jnp.float32)
    residual = (
        hidden_wide
        + attended
        * inverse_rms(jnp.sum(attended * attended, axis=1, keepdims=True), features)
        * post_gain.astype(jnp.float32)
    ).astype(jnp.bfloat16)
    residual_wide = residual.astype(jnp.float32)
    ffn_in = (
        residual_wide
        * inverse_rms(jnp.sum(residual_wide * residual_wide, axis=1, keepdims=True), features)
        * ffn_gain.astype(jnp.float32)
    ).astype(jnp.bfloat16)
    pick_count = expert_ids.shape[1]
    local_experts = gate_experts.shape[0]
    experts_total = local_experts * ep_count
    capacity = max(2, (2 * pick_count * sequences + experts_total - 1) // experts_total)
    flat_ids = expert_ids.reshape(-1)
    choose = (flat_ids[:, None] == lax.broadcasted_iota(jnp.int32, (1, experts_total), 1)).astype(
        jnp.int32
    )
    earlier = jnp.cumsum(choose, axis=0) - choose
    slot_of = jnp.sum(earlier * choose, axis=1)
    target = (flat_ids * capacity + slot_of).reshape(sequences, pick_count)
    slot_iota = lax.broadcasted_iota(jnp.int32, (experts_total * capacity, 1, 1), 0)
    placing = jnp.any(slot_iota == target[None, :, :], axis=2).astype(jnp.bfloat16)
    outgoing = jnp.dot(placing, ffn_in, preferred_element_type=jnp.float32).astype(jnp.bfloat16)
    outgoing = outgoing.reshape(ep_count, local_experts, capacity, features)
    arrived = lax.all_to_all(outgoing, "ep", split_axis=0, concat_axis=0, tiled=True)
    gate_act = jnp.einsum(
        "nlcd,ldf->nlcf", arrived, gate_experts, preferred_element_type=jnp.float32
    )
    up_act = jnp.einsum("nlcd,ldf->nlcf", arrived, up_experts, preferred_element_type=jnp.float32)
    active = (jax.nn.silu(gate_act) * up_act).astype(jnp.bfloat16)
    partial_out = jnp.einsum(
        "nlcf,lfd->nlcd", active, down_experts, preferred_element_type=jnp.float32
    )
    summed = lax.psum_scatter(partial_out, "tp", scatter_dimension=3, tiled=True).astype(
        jnp.bfloat16
    )
    returned = lax.all_to_all(summed, "ep", split_axis=0, concat_axis=0, tiled=True)
    result_table = returned.reshape(experts_total * capacity, slice_width)
    selector = (
        target.reshape(-1)[:, None]
        == lax.broadcasted_iota(jnp.int32, (1, experts_total * capacity), 1)
    ).astype(jnp.bfloat16)
    picked = jnp.dot(selector, result_table, preferred_element_type=jnp.float32)
    picked = picked.reshape(sequences, pick_count, slice_width)
    route_weight = jax.nn.softmax(route_logits, axis=1)
    combined = jnp.sum(route_weight[:, :, None] * picked, axis=1)
    squares = lax.psum(jnp.sum(combined * combined, axis=1), "tp")
    own_residual = lax.dynamic_slice_in_dim(residual_wide, tp_place * slice_width, slice_width, 1)
    result = own_residual + combined * inverse_rms(squares, features)[:, None] * out_gain.astype(
        jnp.float32
    )
    return result.astype(jnp.bfloat16)


def solution(mesh):
    placed = (
        P("ep", None),
        P(),
        P("ep", "tp"),
        P("ep", "tp", None),
        P("ep", "tp", None),
        P("ep"),
        P("tp"),
        P("tp", "ep"),
        P(),
        P(),
        P("ep", None),
        P("ep", None),
        P("ep", None, "tp"),
        P("ep", None, "tp"),
        P("ep", "tp", None),
        P("tp"),
    )
    return jax.shard_map(
        per_device, mesh=mesh, in_specs=placed, out_specs=P("ep", "tp"), check_vma=False
    )
```

profile of v0, /device:TPU:0, one launch (start us, length us, event | category | flops | bytes accessed | tf_op | source)
XLA Modules:
  0.0 194.4 jit_solution(17033841998764324074)
XLA Ops:
  6.5 0.0 copy-start
  6.5 0.0 all-gather.3.cloned.1.call-start
  6.5 0.7 all-gather.3.cloned.1.call-update
  7.3 0.0 all-gather.5.cloned.1.call-start
  7.3 0.7 all-gather.5.cloned.1.call-update
  8.0 0.0 reduce-scatter.2.cloned.1.call-start
  8.1 1.0 fusion.41
  9.0 0.8 copy.51
  9.8 0.1 eq.57
  9.9 0.1 fusion.61
  10.0 0.2 select_reduce_fusion
  10.2 0.1 reduce_sum.69
  10.3 0.1 copy.52
  10.4 0.7 multiply_add_fusion
  11.1 0.1 fusion.60
  11.2 0.7 convert_element_type.60
  11.8 0.7 convert_element_type.67
  12.5 0.7 convert_element_type.71
  13.2 20.8 %all-gather.3.cloned.1.call-done = bf16[2048,256]{1,0:T(8,128)(2,1)} async-done(((bf16[256,256]{1,0:T(8,128)(2,1)}), bf16[2048,256]{1,0:T(8,128)(2,1)}) %all-gather.3.cloned.1.call-update) | async-done | bytes 1048592 | tf_op jit(solution)/shard_map/all_gather | solution.py:65
  34.0 1.5 convolution_convert_fusion.1
  35.5 0.1 reshape.143
  35.6 0.0 copy-start.3
  35.6 0.0 copy-start.4
  35.6 3.7 %fusion.67 = f32[12,4,1,1024]{3,2,1,0:T(1,128)S(1)} fusion(bf16[12,4,64,1]{2,3,1,0:T(2,128)(2,1)S(1)} %reshape.143, bf16[12,4,64,1024]{3,2,1,0:T(8,128)(2,1)} %bitcast.94), kind=kOutput, calls=%fused_computation.78 | convolution fusion | flops 6291456 | bytes 6494208 | tf_op jit(solution)/shard_map/she,shec->shc/dot_general | solution.py:16
  39.4 0.0 copy-done.3
  39.4 0.0 copy-done.4
  39.4 0.3 fusion.29
  39.7 0.1 reshape.123
  39.8 59.4 %reduce-window.6 = f32[12,4,8,128]{3,2,1,0:T(8,128)S(1)} reduce-window(f32[12,4,8,128]{3,2,1,0:T(8,128)S(1)} %reshape.123, f32[]{:T(128)} %constant.13.clone.1), window={size=1x1x1x128 pad=0_0x0_0x0_0x0_127}, to_apply=%region_1.2 | reduce-window | flops 6242304 | bytes 393220 | tf_op jit(solution)/shard_map/reduce-window
  99.2 0.3 copy.49
  99.6 0.1 copy.50
  99.7 0.1 broadcast_add_fusion
  99.8 0.1 reduce_window_sum.26
  99.9 0.6 fusion.50
  100.5 0.0 copy-start.1
  100.6 4.5 %fusion.34 = f32[12,4,1,64]{3,2,1,0:T(1,128)S(1)} fusion(bf16[12,4,64,1024]{3,2,1,0:T(8,128)(2,1)} %bitcast.99, bf16[12,4,1024,1]{2,1,0,3:T(4,128)(2,1)S(1)} %fusion.50), kind=kOutput, calls=%fused_computation.28 | convolution fusion | flops 6291456 | bytes 6402048 | tf_op jit(solution)/shard_map/shc,shec->she/dot_general | solution.py:25
  105.1 0.1 reshape.126
  105.2 0.0 all-gather.5.cloned.1.call-done
  105.2 1.5 fusion.68
  106.7 18.4 %psum.14 = bf16[12,2048]{1,0:T(8,128)(2,1)S(1)} all-reduce(f32[12,2048]{1,0:T(8,128)S(1)} %fusion.68), channel_id=1, replica_groups=mesh['ep'=8,'tp'=4] {'tp'}, use_global_device_ids=true, to_apply=%region_3.4 | all-reduce | flops 24576 | bytes 147456 | tf_op jit(solution)/shard_map/psum | solution.py:78
  125.1 0.1 fusion.39
  125.2 0.0 copy-done.1
  125.2 0.2 multiply_reduce_fusion
  125.5 0.3 convolution_convert_fusion
  125.7 0.1 reshape.127
  125.8 12.7 %all_to_all.10 = bf16[8,1,6,2048]{3,2,1,0:T(8,128)(2,1)S(1)} all-to-all(bf16[8,1,6,2048]{3,2,1,0:T(8,128)(2,1)S(1)} %bitcast.96), channel_id=1, replica_groups=mesh['ep'=8,'tp'=4] {'ep'}, dimensions={0} | all-to-all | bytes 393216 | tf_op jit(solution)/shard_map/all_to_all | solution.py:107
  138.6 2.0 %fusion.5 = f32[8,1,6,512]{3,0,2,1:T(8,128)S(1)} fusion(bf16[1,2048,512]{2,1,0:T(8,128)(2,1)} %param.28, bf16[8,1,6,2048]{3,2,1,0:T(8,128)(2,1)S(1)} %all_to_all.10), kind=kOutput, calls=%fused_computation.7 | convolution fusion | flops 100663296 | bytes 2392064 | tf_op jit(solution)/shard_map/nlcd,ldf->nlcf/dot_general | solution.py:108
  140.6 0.0 copy-done
  140.6 0.0 copy-start.2
  140.6 0.0 copy-start.5
  140.6 3.2 %convolution_bitcast_fusion = f32[8,1,6,2048]{3,0,2,1:T(8,128)} fusion(bf16[1,512,2048]{2,1,0:T(8,128)(2,1)S(1)} %copy-done, bf16[1,2048,512]{2,1,0:T(8,128)(2,1)} %param.29, bf16[8,1,6,2048]{3,2,1,0:T(8,128)(2,1)S(1)} %all_to_all.10, f32[8,1,6,512]{3,0,2,1:T(8,128)S(1)} %fusion.5), kind=kOutput, calls=%fused_computation | convolution fusion | flops 201474048 | bytes 4882432 | tf_op jit(solution)/shard_map/nlcf,lfd->nlcd/dot_general | solution.py:113
  143.8 0.0 reduce-scatter.2.cloned.1.call-update
  143.8 0.0 copy-done.2
  143.8 22.0 %reduce-scatter.2.cloned.1.call-done = f32[8,1,6,512]{3,0,2,1:T(8,128)} async-done(((f32[8,1,6,2048]{3,0,2,1:T(8,128)}), f32[8,1,6,512]{3,0,2,1:T(8,128)}) %reduce-scatter.2.cloned.1.call-update) | async-done | bytes 98320 | tf_op jit(solution)/shard_map/reduce_scatter | solution.py:116
  165.9 0.9 convert_element_type.75
  166.8 0.6 copy.55
  167.4 4.6 %all-to-all-start.1 = ((bf16[8,1,6,512]{3,2,1,0:T(8,128)(2,1)}), bf16[8,1,6,512]{3,2,1,0:T(8,128)(2,1)S(1)}, u32[]{:S(2)}, u32[]{:S(2)}) async-start(bf16[8,1,6,512]{3,2,1,0:T(8,128)(2,1)} %copy.55), calls=%async_computation.2 | async-start | bytes 131072 | tf_op jit(solution)/shard_map/all_to_all | solution.py:119
  172.1 0.0 copy-done.5
  172.1 5.9 %all-to-all-done.1 = bf16[8,1,6,512]{3,2,1,0:T(8,128)(2,1)S(1)} async-done(((bf16[8,1,6,512]{3,2,1,0:T(8,128)(2,1)}), bf16[8,1,6,512]{3,2,1,0:T(8,128)(2,1)S(1)}, u32[]{:S(2)}, u32[]{:S(2)}) %all-to-all-start.1) | async-done | bytes 49184 | tf_op jit(solution)/shard_map/all_to_all | solution.py:119
  178.0 0.2 fusion.17
  178.2 0.1 multiply_reduce_fusion.1
  178.3 8.9 %psum.15 = f32[12]{0:T(128)S(1)} all-reduce(f32[12]{0:T(128)S(1)} %multiply_reduce_fusion.1), channel_id=1, replica_groups=mesh['ep'=8,'tp'=4] {'tp'}, use_global_device_ids=true, to_apply=%region_14.15 | all-reduce | flops 12 | bytes 96 | tf_op jit(solution)/shard_map/psum | solution.py:129
  187.2 0.7 add_convert_fusion
  (13 shorter events, 0.2 us)
Async XLA Ops:
  6.5 134.0 %copy-start = (bf16[1,512,2048]{2,1,0:T(8,128)(2,1)S(1)}, bf16[1,512,2048]{2,1,0:T(8,128)(2,1)}, u32[]{:S(2)}) copy-start(bf16[1,512,2048]{2,1,0:T(8,128)(2,1)} %param.30) | copy-start | bytes 6291460
  6.5 27.4 %all-gather.3.cloned.1.call-start = ((), (), s32[]{:S(2)}) async-start(), calls=%async_computation.3 | async-start | bytes 1179648 | tf_op jit(solution)/shard_map/all_gather | solution.py:65
  7.3 97.9 %all-gather.5.cloned.1.call-start = ((), (), s32[]{:S(2)}) async-start(), calls=%async_computation.4 | async-start | bytes 1179648 | tf_op jit(solution)/shard_map/all_gather | solution.py:75
  8.0 157.9 %reduce-scatter.2.cloned.1.call-start = ((), (), s32[]{:S(2)}) async-start(), calls=%async_computation.5 | async-start | bytes 491520 | tf_op jit(solution)/shard_map/reduce_scatter | solution.py:116
  35.6 3.8 %copy-start.3 = (f32[4]{0:T(128)S(1)}, f32[4]{0:T(128)}, u32[]{:S(2)}) copy-start(f32[4]{0:T(128)} %param.22) | copy-start | bytes 52
  35.6 3.8 %copy-start.4 = (s32[12]{0:T(128)S(1)}, s32[12]{0:T(128)}, u32[]{:S(2)}) copy-start(s32[12]{0:T(128)} %param.21) | copy-start | bytes 148
  100.5 24.7 %copy-start.1 = (bf16[12,2048]{1,0:T(8,128)(2,1)S(1)}, bf16[12,2048]{1,0:T(8,128)(2,1)}, u32[]{:S(2)}) copy-start(bf16[12,2048]{1,0:T(8,128)(2,1)} %param.16) | copy-start | bytes 147460
  140.6 3.2 %copy-start.2 = (f32[12,2]{0,1:T(2,128)S(1)}, f32[12,2]{0,1:T(2,128)}, u32[]{:S(2)}) copy-start(f32[12,2]{0,1:T(2,128)} %param.27) | copy-start | bytes 292
  140.6 31.5 %copy-start.5 = (bf16[512]{0:T(512)(128)(2,1)S(1)}, bf16[512]{0:T(512)(128)(2,1)}, u32[]{:S(2)}) copy-start(bf16[512]{0:T(512)(128)(2,1)} %param.31) | copy-start | bytes 3076
  167.4 10.5 %all-to-all-start.1 = ((bf16[8,1,6,512]{3,2,1,0:T(8,128)(2,1)}), bf16[8,1,6,512]{3,2,1,0:T(8,128)(2,1)S(1)}, u32[]{:S(2)}, u32[]{:S(2)}) async-start(bf16[8,1,6,512]{3,2,1,0:T(8,128)(2,1)} %copy.55), calls=%async_computation.2 | async-start | bytes 131072 | tf_op jit(solution)/shard_map/all_to_all | solution.py:119
Sparse Core Ops, SparseCore 0:
  8.9 25.0 all-gather.2
  35.6 23.5 all-gather.4
  143.9 21.9 reduce-scatter.1
where the time goes:
time: 195 us; the launch traced here: 194 us
  other arithmetic  66.8 us (34%)
  waiting for transfers between devices  50.1 us (26%)
  blocking collectives  40.1 us (21%)
  matrix products  16.9 us (9%)
  between operations  13.3 us (7%)
  starting transfers between devices  4.69 us (2%)
  local copies, waits for them, and re-layouts  2.53 us (1%)
    another operation x2, other arithmetic  59.5 us
    reduce_scatter x1, waiting for transfers between devices, per_device(): lax.psum_scatter(partial_out, 'tp', scatter_dimension=3, tiled=True)  22 us
    all_gather x1, waiting for transfers between devices, per_device(): lax.all_gather(query_weight, 'ep', axis=0, tiled=True)  20.8 us
    psum x1, blocking collectives, per_device(): attended = lax.psum(partial_value, 'tp').astype(jnp.bfloat16)  18.4 us
    all_to_all x1, blocking collectives, per_device(): lax.all_to_all(outgoing, 'ep', split_axis=0, concat_axis=0, tiled=True)  12.7 us
    psum x1, blocking collectives, per_device(): squares = lax.psum(jnp.sum(combined * combined, axis=1), 'tp')  8.93 us
    all_to_all x1, waiting for transfers between devices, per_device(): lax.all_to_all(summed, 'ep', split_axis=0, concat_axis=0, tiled=True)  5.88 us
    all_to_all x1, starting transfers between devices, per_device(): lax.all_to_all(summed, 'ep', split_axis=0, concat_axis=0, tiled=True)  4.61 us
  transfers between devices with their start and end apart: 4, of which 3 were waited for; matrix products, arithmetic and copies ran while one was open for 39% of the time, Pallas kernels for 0%

commit v1 on v0

--- a/solution.py
+++ b/solution.py
@@ -75,7 +75,7 @@
         lax.all_gather(out_weight, "ep", axis=1, tiled=True),
         preferred_element_type=jnp.float32,
     )
-    attended = lax.psum(partial_value, "tp").astype(jnp.bfloat16)
+    attended = jnp.sum(lax.all_gather(partial_value, "tp"), axis=0).astype(jnp.bfloat16)
     attended = lax.optimization_barrier(attended).astype(jnp.float32)
     residual = (
         hidden_wide

time: 195 us -> 187 us (0.959)
  blocking collectives: 40.1 us -> 31.7 us
    psum x1 -> x0, blocking collectives: 18.4 us -> none  [per_device(): attended = lax.psum(partial_value, 'tp').astype(jnp.bfloat16)]
    all_gather x0 -> x1, blocking collectives: none -> 10 us  [per_device(): lax.all_gather(partial_value, 'tp')]
  transfers between devices with their start and end apart: 4 -> 4, of which waited for: 3 -> 3; matrix products, arithmetic and copies ran while one was open for 39% -> 41% of each run, Pallas kernels for 0% -> 0%
where the time goes in v1:
time: 187 us
  other arithmetic  66.9 us (36%)
  waiting for transfers between devices  50.9 us (27%)
  blocking collectives  31.7 us (17%)
  matrix products  16.9 us (9%)
  between operations  13.3 us (7%)
  starting transfers between devices  4.69 us (3%)
  local copies, waits for them, and re-layouts  2.52 us (1%)
    another operation x2, other arithmetic  59.5 us
    reduce_scatter x1, waiting for transfers between devices, per_device(): lax.psum_scatter(partial_out, 'tp', scatter_dimension=3, tiled=True)  22.8 us
    all_gather x1, waiting for transfers between devices, per_device(): lax.all_gather(query_weight, 'ep', axis=0, tiled=True)  20.8 us
    all_to_all x1, blocking collectives, per_device(): lax.all_to_all(outgoing, 'ep', split_axis=0, concat_axis=0, tiled=True)  12.8 us
    all_gather x1, blocking collectives, per_device(): lax.all_gather(partial_value, 'tp')  10 us
    psum x1, blocking collectives, per_device(): squares = lax.psum(jnp.sum(combined * combined, axis=1), 'tp')  8.92 us
    all_to_all x1, waiting for transfers between devices, per_device(): lax.all_to_all(summed, 'ep', split_axis=0, concat_axis=0, tiled=True)  5.88 us
    all_to_all x1, starting transfers between devices, per_device(): lax.all_to_all(summed, 'ep', split_axis=0, concat_axis=0, tiled=True)  4.61 us
  transfers between devices with their start and end apart: 4, of which 3 were waited for; matrix products, arithmetic and copies ran while one was open for 41% of the time, Pallas kernels for 0%

profile of v1, /device:TPU:0, one launch (start us, length us, event | category | flops | bytes accessed | tf_op | source)
XLA Modules:
  0.0 186.8 jit_solution(9585491430346848270)
XLA Ops:
  6.5 0.0 copy-start
  6.5 0.0 all-gather.5.cloned.1.call-start
  6.5 0.7 all-gather.5.cloned.1.call-update
  7.3 0.0 all-gather.7.cloned.1.call-start
  7.3 0.7 all-gather.7.cloned.1.call-update
  8.0 0.0 reduce-scatter.2.cloned.1.call-start
  8.1 1.0 fusion.41
  9.0 0.8 copy.51
  9.8 0.1 eq.57
  9.9 0.1 fusion.61
  10.0 0.2 select_reduce_fusion
  10.2 0.1 reduce_sum.79
  10.3 0.1 copy.52
  10.4 0.7 multiply_add_fusion
  11.1 0.1 fusion.60
  11.2 0.7 convert_element_type.60
  11.8 0.7 convert_element_type.67
  12.5 0.7 convert_element_type.71
  13.2 20.8 %all-gather.5.cloned.1.call-done = bf16[2048,256]{1,0:T(8,128)(2,1)} async-done(((bf16[256,256]{1,0:T(8,128)(2,1)}), bf16[2048,256]{1,0:T(8,128)(2,1)}) %all-gather.5.cloned.1.call-update) | async-done | bytes 1048592 | tf_op jit(solution)/shard_map/all_gather | solution.py:65
  34.0 1.5 convolution_convert_fusion.1
  35.5 0.1 reshape.147
  35.6 0.0 copy-start.3
  35.6 0.0 copy-start.4
  35.6 3.7 %fusion.67 = f32[12,4,1,1024]{3,2,1,0:T(1,128)S(1)} fusion(bf16[12,4,64,1]{2,3,1,0:T(2,128)(2,1)S(1)} %reshape.147, bf16[12,4,64,1024]{3,2,1,0:T(8,128)(2,1)} %bitcast.96), kind=kOutput, calls=%fused_computation.79 | convolution fusion | flops 6291456 | bytes 6494208 | tf_op jit(solution)/shard_map/she,shec->shc/dot_general | solution.py:16
  39.4 0.0 copy-done.3
  39.4 0.0 copy-done.4
  39.4 0.3 fusion.29
  39.7 0.1 reshape.123
  39.8 59.4 %reduce-window.6 = f32[12,4,8,128]{3,2,1,0:T(8,128)S(1)} reduce-window(f32[12,4,8,128]{3,2,1,0:T(8,128)S(1)} %reshape.123, f32[]{:T(128)} %constant.13.clone.1), window={size=1x1x1x128 pad=0_0x0_0x0_0x0_127}, to_apply=%region_1.2 | reduce-window | flops 6242304 | bytes 393220 | tf_op jit(solution)/shard_map/reduce-window
  99.2 0.3 copy.49
  99.6 0.1 copy.50
  99.7 0.1 broadcast_add_fusion
  99.8 0.1 reduce_window_sum.26
  99.9 0.6 fusion.50
  100.5 4.5 %fusion.34 = f32[12,4,1,64]{3,2,1,0:T(1,128)S(1)} fusion(bf16[12,4,64,1024]{3,2,1,0:T(8,128)(2,1)} %bitcast.101, bf16[12,4,1024,1]{2,1,0,3:T(4,128)(2,1)S(1)} %fusion.50), kind=kOutput, calls=%fused_computation.29 | convolution fusion | flops 6291456 | bytes 6402048 | tf_op jit(solution)/shard_map/shc,shec->she/dot_general | solution.py:25
  105.1 0.0 copy-start.1
  105.1 0.1 reshape.126
  105.2 0.0 all-gather.7.cloned.1.call-done
  105.2 1.5 convolution_bitcast_fusion.1
  106.7 10.0 %all-gather.1 = f32[4,12,2048]{2,1,0:T(8,128)S(1)} all-gather(f32[1,12,2048]{2,1,0:T(8,128)S(1)} %convolution_bitcast_fusion.1), channel_id=2, replica_groups=mesh['ep'=8,'tp'=4] {'tp'}, dimensions={0}, use_global_device_ids=true | all-gather | bytes 491520 | tf_op jit(solution)/shard_map/all_gather | solution.py:78
  116.7 0.1 fusion.39
  116.8 0.0 copy-done.1
  116.8 0.2 multiply_reduce_fusion
  117.1 0.3 convolution_convert_fusion
  117.3 0.1 reshape.127
  117.4 12.8 %all_to_all.10 = bf16[8,1,6,2048]{3,2,1,0:T(8,128)(2,1)S(1)} all-to-all(bf16[8,1,6,2048]{3,2,1,0:T(8,128)(2,1)S(1)} %bitcast.98), channel_id=1, replica_groups=mesh['ep'=8,'tp'=4] {'ep'}, dimensions={0} | all-to-all | bytes 393216 | tf_op jit(solution)/shard_map/all_to_all | solution.py:107
  130.2 2.0 %fusion.5 = f32[8,1,6,512]{3,0,2,1:T(8,128)S(1)} fusion(bf16[1,2048,512]{2,1,0:T(8,128)(2,1)} %param.28, bf16[8,1,6,2048]{3,2,1,0:T(8,128)(2,1)S(1)} %all_to_all.10), kind=kOutput, calls=%fused_computation.8 | convolution fusion | flops 100663296 | bytes 2392064 | tf_op jit(solution)/shard_map/nlcd,ldf->nlcf/dot_general | solution.py:108
  132.2 0.0 copy-done
  132.2 0.0 copy-start.2
  132.2 0.0 copy-start.5
  132.2 3.2 %convolution_bitcast_fusion = f32[8,1,6,2048]{3,0,2,1:T(8,128)} fusion(bf16[1,512,2048]{2,1,0:T(8,128)(2,1)S(1)} %copy-done, bf16[1,2048,512]{2,1,0:T(8,128)(2,1)} %param.29, bf16[8,1,6,2048]{3,2,1,0:T(8,128)(2,1)S(1)} %all_to_all.10, f32[8,1,6,512]{3,0,2,1:T(8,128)S(1)} %fusion.5), kind=kOutput, calls=%fused_computation | convolution fusion | flops 201474048 | bytes 4882432 | tf_op jit(solution)/shard_map/nlcf,lfd->nlcd/dot_general | solution.py:113
  135.4 0.0 reduce-scatter.2.cloned.1.call-update
  135.4 0.0 copy-done.2
  135.5 22.8 %reduce-scatter.2.cloned.1.call-done = f32[8,1,6,512]{3,0,2,1:T(8,128)} async-done(((f32[8,1,6,2048]{3,0,2,1:T(8,128)}), f32[8,1,6,512]{3,0,2,1:T(8,128)}) %reduce-scatter.2.cloned.1.call-update) | async-done | bytes 98320 | tf_op jit(solution)/shard_map/reduce_scatter | solution.py:116
  158.3 0.9 convert_element_type.75
  159.2 0.6 copy.55
  159.8 4.6 %all-to-all-start.1 = ((bf16[8,1,6,512]{3,2,1,0:T(8,128)(2,1)}), bf16[8,1,6,512]{3,2,1,0:T(8,128)(2,1)S(1)}, u32[]{:S(2)}, u32[]{:S(2)}) async-start(bf16[8,1,6,512]{3,2,1,0:T(8,128)(2,1)} %copy.55), calls=%async_computation.2 | async-start | bytes 131072 | tf_op jit(solution)/shard_map/all_to_all | solution.py:119
  164.4 0.0 copy-done.5
  164.5 5.9 %all-to-all-done.1 = bf16[8,1,6,512]{3,2,1,0:T(8,128)(2,1)S(1)} async-done(((bf16[8,1,6,512]{3,2,1,0:T(8,128)(2,1)}), bf16[8,1,6,512]{3,2,1,0:T(8,128)(2,1)S(1)}, u32[]{:S(2)}, u32[]{:S(2)}) %all-to-all-start.1) | async-done | bytes 49184 | tf_op jit(solution)/shard_map/all_to_all | solution.py:119
  170.4 0.2 fusion.17
  170.6 0.1 multiply_reduce_fusion.1
  170.7 8.9 %psum.7 = f32[12]{0:T(128)S(1)} all-reduce(f32[12]{0:T(128)S(1)} %multiply_reduce_fusion.1), channel_id=1, replica_groups=mesh['ep'=8,'tp'=4] {'tp'}, use_global_device_ids=true, to_apply=%region_14.15 | all-reduce | flops 12 | bytes 96 | tf_op jit(solution)/shard_map/psum | solution.py:129
  179.6 0.7 add_convert_fusion
  (14 shorter events, 0.3 us)
Async XLA Ops:
  6.5 125.7 %copy-start = (bf16[1,512,2048]{2,1,0:T(8,128)(2,1)S(1)}, bf16[1,512,2048]{2,1,0:T(8,128)(2,1)}, u32[]{:S(2)}) copy-start(bf16[1,512,2048]{2,1,0:T(8,128)(2,1)} %param.30) | copy-start | bytes 6291460
  6.5 27.4 %all-gather.5.cloned.1.call-start = ((), (), s32[]{:S(2)}) async-start(), calls=%async_computation.3 | async-start | bytes 1179648 | tf_op jit(solution)/shard_map/all_gather | solution.py:65
  7.3 97.9 %all-gather.7.cloned.1.call-start = ((), (), s32[]{:S(2)}) async-start(), calls=%async_computation.4 | async-start | bytes 1179648 | tf_op jit(solution)/shard_map/all_gather | solution.py:75
  8.0 150.3 %reduce-scatter.2.cloned.1.call-start = ((), (), s32[]{:S(2)}) async-start(), calls=%async_computation.5 | async-start | bytes 491520 | tf_op jit(solution)/shard_map/reduce_scatter | solution.py:116
  35.6 3.8 %copy-start.3 = (f32[4]{0:T(128)S(1)}, f32[4]{0:T(128)}, u32[]{:S(2)}) copy-start(f32[4]{0:T(128)} %param.22) | copy-start | bytes 52
  35.6 3.8 %copy-start.4 = (s32[12]{0:T(128)S(1)}, s32[12]{0:T(128)}, u32[]{:S(2)}) copy-start(s32[12]{0:T(128)} %param.21) | copy-start | bytes 148
  105.1 11.8 %copy-start.1 = (bf16[12,2048]{1,0:T(8,128)(2,1)S(1)}, bf16[12,2048]{1,0:T(8,128)(2,1)}, u32[]{:S(2)}) copy-start(bf16[12,2048]{1,0:T(8,128)(2,1)} %param.16) | copy-start | bytes 147460
  132.2 3.2 %copy-start.2 = (f32[12,2]{0,1:T(2,128)S(1)}, f32[12,2]{0,1:T(2,128)}, u32[]{:S(2)}) copy-start(f32[12,2]{0,1:T(2,128)} %param.27) | copy-start | bytes 292
  132.2 32.2 %copy-start.5 = (bf16[512]{0:T(512)(128)(2,1)S(1)}, bf16[512]{0:T(512)(128)(2,1)}, u32[]{:S(2)}) copy-start(bf16[512]{0:T(512)(128)(2,1)} %param.31) | copy-start | bytes 3076
  159.8 10.5 %all-to-all-start.1 = ((bf16[8,1,6,512]{3,2,1,0:T(8,128)(2,1)}), bf16[8,1,6,512]{3,2,1,0:T(8,128)(2,1)S(1)}, u32[]{:S(2)}, u32[]{:S(2)}) async-start(bf16[8,1,6,512]{3,2,1,0:T(8,128)(2,1)} %copy.55), calls=%async_computation.2 | async-start | bytes 131072 | tf_op jit(solution)/shard_map/all_to_all | solution.py:119
Sparse Core Ops, SparseCore 0:
  8.9 25.0 all-gather.4
  35.6 23.5 all-gather.6
  135.5 22.6 reduce-scatter.1
